TPU v7x, 512 devices: a 4x2x32 block of a 4x8x32 slice. The times are simulated.
512 devices in a mesh: grp: 2 (over y), sp: 64 (over z, core), tp: 4 (over x).
Axes of the slice: x: 4, y: 2, z: 32, core: 2. Of those that a mesh axis runs over, the one named last changes fastest.
The devices are a block of a 4x8x32 slice.
Arguments:
- tokens: bfloat16 [20480, 2048], P(('grp', 'sp')), parts along dimension 0, may hold values from -6 to 6
- norm_gain: float32 [2048], replicated, may hold values from 0.6 to 5
- query_weight: bfloat16 [2048, 2048], P('sp', 'tp')
- key_weight: bfloat16 [2048, 512], P('sp', 'tp')
- value_weight: bfloat16 [2048, 512], P('sp', 'tp'), may hold values from -0.125 to 0.125
- map_lambda: float32 [16], P('tp'), may hold values from 0.3 to 0.8
- head_gain: float32 [16, 128], P('tp'), may hold values from 0.1 to 1.9
- attn_out_weight: bfloat16 [2048, 2048], P('tp', 'sp'), may hold values from -0.125 to 0.125
- pool_out_weight: bfloat16 [2048, 2048], P('tp', 'sp'), may hold values from -0.09375 to 0.09375
Outputs:
- mixed_rows: bfloat16 [20480, 2048], P(('grp', 'sp', 'tp')), parts along dimension 0
- log_totals: float32 [2, 16, 20480], P(None, 'tp', ('grp', 'sp')), parts along dimension 2
There are 2 independent parts, one for each index of `grp`. A program takes and returns all parts, laid end to end along the dimension named above; an argument that names none is the same for every part. Nothing has to cross between parts.
All inputs are finite; a program needn't handle non-finite values.
Results may differ from a plain program's by a relative error of at most 0.013.
The roundings to bfloat16 on the way count: a program that leaves them out, or rounds other values in their place, can miss the bound.
Values may be sent and summed in bfloat16 or wider, within the bound.
No kernel may reach another device: no remote copies, remote signals or barrier semaphores. Data moves between devices by JAX's collectives and lax.ppermute only.
A program may use at most 64 MiB of HBM per device.

v0:
```python
import math
import jax
import jax.numpy as jnp
from jax import lax
from jax.sharding import PartitionSpec as P

HD = 64
VD = 128
POOL_SPAN = 16
epsilon = 1e-06
very_low = -1e30


def extended(cells, sides, width):
    for axis, dim in sides:
        count = lax.axis_size(axis)
        ends = count - 1
        head = lax.slice_in_dim(cells, 0, width, axis=dim)
        tail = lax.slice_in_dim(cells, cells.shape[dim] - width, cells.shape[dim], axis=dim)
        cells = jnp.concatenate(
            [
                lax.ppermute(tail, axis, [(i, (i + 1) % count) for i in range(ends)]),
                cells,
                lax.ppermute(head, axis, [((i + 1) % count, i) for i in range(ends)]),
            ],
            axis=dim,
        )
    return cells


def side_by_side(arrays, axis, dim, along):
    both = jnp.concatenate(arrays, axis=along)
    whole, at, gathered = (lax.all_gather(both, axis, axis=dim, tiled=True), 0, [])
    for a in arrays:
        gathered.append(lax.slice_in_dim(whole, at, at + a.shape[along], axis=along))
        at += a.shape[along]
    return tuple(gathered)


def rows_first(arrays, axis, dims):
    turned = [jnp.moveaxis(a, dim, 0) for a, dim in zip(arrays, dims)]
    widths = [t[0].size for t in turned]
    both = jnp.concatenate([t.reshape(-1, w) for t, w in zip(turned, widths)], axis=1)
    whole = lax.all_gather(both, axis, axis=0, tiled=True)
    blocks = jnp.split(whole, [sum(widths[:k]) for k in range(1, len(widths))], axis=1)
    return tuple(
        (
            jnp.moveaxis(b.reshape(-1, *t.shape[1:]), 0, dim)
            for b, t, dim in zip(blocks, turned, dims)
        )
    )


def cut_along(x, dim, length):
    before, after = (x.shape[:dim], x.shape[dim + 1 :])
    return jnp.moveaxis(x.reshape(*before, length, -1, *after), dim, 0)


def sent_and_summed(x, axis, dim):
    blocks = cut_along(x, dim, lax.axis_size(axis))
    arrived = lax.all_to_all(blocks, axis, split_axis=0, concat_axis=0, tiled=True)
    return arrived.astype(jnp.float32).sum(axis=0)


def add_products(totals, pieces, source):
    results = []
    for running, piece in zip(totals, pieces):
        results.append(jnp.dot(source, piece, preferred_element_type=jnp.float32))
    return tuple(results)


def on_device(
    tokens,
    norm_gain,
    query_weight,
    key_weight,
    value_weight,
    map_lambda,
    head_gain,
    attn_out_weight,
    pool_out_weight,
):
    tokens_wide = tokens.astype(jnp.float32)
    normed = (
        tokens_wide
        * lax.rsqrt(jnp.mean(tokens_wide * tokens_wide, axis=-1, keepdims=True) + epsilon)
        * norm_gain
    ).astype(jnp.bfloat16)
    row_count = normed.shape[0]
    sp_index = lax.axis_index("sp")
    tp_index = lax.axis_index("tp")
    group_width = pool_out_weight.shape[0]
    local_heads = map_lambda.shape[0]
    key_heads = value_weight.shape[1] // VD
    group_heads = local_heads // key_heads
    q_empty = jnp.zeros((row_count, query_weight.shape[1]), jnp.float32)
    k_empty = jnp.zeros((row_count, key_weight.shape[1]), jnp.float32)
    v_empty = jnp.zeros((row_count, value_weight.shape[1]), jnp.float32)
    q_acc, k_acc, v_acc = add_products(
        (q_empty, k_empty, v_empty),
        side_by_side((query_weight, key_weight, value_weight), "sp", 0, 1),
        normed,
    )
    queries = q_acc.astype(jnp.bfloat16).reshape(row_count, key_heads, group_heads, 2, HD)
    keys_flat = k_acc.astype(jnp.bfloat16)
    values_flat = v_acc.astype(jnp.bfloat16)

    def key_block(state_now, key_pair):
        maxima, totals, accums = state_now
        key_blk, val_blk = key_pair
        scores = jnp.einsum(
            "qhgmd,khmd->hgmqk", queries, key_blk, preferred_element_type=jnp.float32
        ) * HD ** (-0.5)
        highest = jnp.maximum(maxima, jnp.max(scores, axis=-1))
        factor = jnp.exp(maxima - highest)
        weights = jnp.exp(scores - highest[..., None])
        totals = totals * factor + jnp.sum(weights, axis=-1)
        accums = accums * factor[..., None] + jnp.einsum(
            "hgmqk,khe->hgmqe",
            weights.astype(jnp.bfloat16),
            val_blk,
            preferred_element_type=jnp.float32,
        )
        return ((highest, totals, accums), None)

    start_state = (
        jnp.full((key_heads, group_heads, 2, row_count), very_low, jnp.float32),
        jnp.zeros((key_heads, group_heads, 2, row_count), jnp.float32),
        jnp.zeros((key_heads, group_heads, 2, row_count, VD), jnp.float32),
    )
    key_piece, val_piece = side_by_side((keys_flat, values_flat), "sp", 0, 1)
    piece_len = key_piece.shape[0]
    block_len = math.gcd(piece_len, 512)
    key_blocks = key_piece.reshape(piece_len // block_len, block_len, key_heads, 2, HD)
    val_blocks = val_piece.reshape(piece_len // block_len, block_len, key_heads, VD)
    state_next, unused = lax.scan(key_block, start_state, (key_blocks, val_blocks))
    maxima, totals, accums = state_next
    log_parts = maxima + jnp.log(totals)
    log_totals = jnp.transpose(log_parts, (2, 0, 1, 3)).reshape(2, local_heads, row_count)
    reads = accums / totals[..., None]
    contrast = reads[:, :, 0] - map_lambda.reshape(key_heads, group_heads, 1, 1) * reads[:, :, 1]
    scaled = (
        contrast
        * lax.rsqrt(jnp.mean(contrast * contrast, axis=-1, keepdims=True) + epsilon)
        * head_gain.reshape(key_heads, group_heads, 1, VD)
    )
    attention_head_rows = (
        jnp.transpose(scaled, (2, 0, 1, 3))
        .reshape(row_count, local_heads * VD)
        .astype(jnp.bfloat16)
    )
    head_rows, log_totals = (attention_head_rows, log_totals)
    own_chan = lax.dynamic_slice_in_dim(normed, tp_index * group_width, group_width, 1)
    reach = POOL_SPAN // 2
    padded = extended(own_chan, (("sp", 0),), reach)
    window = jnp.left_shift(jnp.int32(2), tp_index)
    half_span = window // 2
    running = jnp.zeros((row_count, group_width), jnp.float32)
    for offset in range(POOL_SPAN):
        piece = lax.dynamic_slice_in_dim(padded, reach - half_span + offset, row_count, 0).astype(
            jnp.float32
        )
        running = running + jnp.where(offset < window, piece, 0.0)
    seq_len = row_count * lax.axis_size("sp")
    position = sp_index * row_count + jnp.arange(row_count, dtype=jnp.int32)
    lower_edge = jnp.clip(position - half_span, 0, seq_len)
    upper_edge = jnp.clip(position + window - half_span, 0, seq_len)
    counts_f = (upper_edge - lower_edge).astype(jnp.float32)[:, None]
    pooled = (running / counts_f - own_chan.astype(jnp.float32)).astype(jnp.bfloat16)
    attn_whole, pool_whole = rows_first((attn_out_weight, pool_out_weight), "sp", (1, 1))
    mixed = sent_and_summed(
        (
            jnp.dot(head_rows, attn_whole, preferred_element_type=jnp.float32)
            + jnp.dot(pooled, pool_whole, preferred_element_type=jnp.float32)
        ).astype(jnp.bfloat16),
        "tp",
        0,
    )
    return (mixed.astype(jnp.bfloat16), log_totals)


def solution(mesh):
    placed = (
        P(("grp", "sp"), None),
        P(),
        P("sp", "tp"),
        P("sp", "tp"),
        P("sp", "tp"),
        P("tp"),
        P("tp", None),
        P("tp", "sp"),
        P("tp", "sp"),
    )
    return jax.shard_map(
        on_device,
        mesh=mesh,
        in_specs=placed,
        out_specs=(P(("grp", "sp", "tp"), None), P(None, "tp", ("grp", "sp"))),
        check_vma=False,
    )
```

profile of v0, /device:TPU:33, one launch (start us, length us, event | category | flops | bytes accessed | tf_op | source)
XLA Modules:
  0.0 463.9 jit_solution(1996531351021676169)
XLA Ops:
  11.4 161.0 %all-gather.4.cloned.1.call-done = bf16[2048,768]{1,0:T(8,128)(2,1)} async-done(((bf16[32,768]{1,0:T(8,128)(2,1)}), bf16[2048,768]{1,0:T(8,128)(2,1)}) %all-gather.4.cloned.1.call-update) | async-done | bytes 3145744 | tf_op jit(solution)/shard_map/all_gather | solution.py:33
  176.0 2.4 collective-permute-start
  178.4 2.0 collective-permute-start.1
  184.1 2.1 fusion.30
  186.4 118.8 %all-gather.6.cloned.1.call-done = bf16[10240,256]{1,0:T(8,128)(2,1)} async-done(((bf16[160,256]{1,0:T(8,128)(2,1)}), bf16[10240,256]{1,0:T(8,128)(2,1)}) %all-gather.6.cloned.1.call-update) | async-done | bytes 5242896 | tf_op jit(solution)/shard_map/all_gather | solution.py:33
  305.2 3.7 fusion.76
  308.9 4.2 reshape.146
  313.2 11.1 %copy.22 = bf16[20,512,1,2,64]{1,4,3,2,0:T(8,128)(2,1)} copy(bf16[20,512,1,2,64]{4,3,1,0,2:T(2,128)(2,1)} %reshape.146) | data formatting | bytes 5242880
  324.3 90.8 %while.15 = (s32[]{:T(128)}, f32[1,4,2,160]{3,1,2,0:T(4,128)S(1)}, f32[1,4,2,160]{3,1,2,0:T(4,128)}, f32[1,4,2,160,128]{4,3,2,1,0:T(8,128)S(1)}, bf16[20,512,1,2...) while((s32[]{:T(128)}, f32[1,4,2,160]{3,1,2,0:T(4,128)S(1)}, ...), condition=%wide.region_4.5_spmd.clone, body=%wide.region_1.4_spmd.clone.sunk | while | flops 256089600 | bytes 9730209 | solution.py:136
  324.3 1.6 bitcast_reduce_fusion.2
  328.8 1.6 bitcast_reduce_fusion.2
  333.4 1.6 bitcast_reduce_fusion.2
  337.9 1.6 bitcast_reduce_fusion.2
  342.5 1.6 bitcast_reduce_fusion.2
  347.0 1.6 bitcast_reduce_fusion.2
  351.6 1.6 bitcast_reduce_fusion.2
  356.1 1.6 bitcast_reduce_fusion.2
  360.7 1.6 bitcast_reduce_fusion.2
  365.2 1.6 bitcast_reduce_fusion.2
  369.7 1.6 bitcast_reduce_fusion.2
  374.3 1.6 bitcast_reduce_fusion.2
  378.8 1.6 bitcast_reduce_fusion.2
  383.4 1.6 bitcast_reduce_fusion.2
  387.9 1.6 bitcast_reduce_fusion.2
  397.0 1.6 bitcast_reduce_fusion.2
  401.5 1.6 bitcast_reduce_fusion.2
  406.1 1.6 bitcast_reduce_fusion.2
  418.1 17.0 %all-gather.8.cloned.1.call-done = bf16[2048,1024]{1,0:T(8,128)(2,1)} async-done(((bf16[32,1024]{1,0:T(8,128)(2,1)}), bf16[2048,1024]{1,0:T(8,128)(2,1)}) %all-gather.8.cloned.1.call-update) | async-done | bytes 4194320 | tf_op jit(solution)/shard_map/all_gather | solution.py:44
  435.1 2.4 fusion.23
  437.6 4.5 fusion.21
  442.1 4.1 all-to-all-start
  446.8 9.8 %all-to-all-done = bf16[4,40,2048]{2,1,0:T(8,128)(2,1)S(1)} async-done(((bf16[4,40,2048]{2,1,0:T(8,128)(2,1)}), bf16[4,40,2048]{2,1,0:T(8,128)(2,1)S(1)}, u32[]{:S(2)}, u32[]{:S(2)}) %all-to-all-start) | async-done | bytes 655392 | tf_op jit(solution)/shard_map/all_to_all | solution.py:61
  (249 shorter events, 75.9 us)
Async XLA Ops:
  7.2 173.2 %copy-start.7 = (bf16[512,32]{0,1:T(8,128)(2,1)S(1)}, bf16[512,32]{0,1:T(8,128)(2,1)}, u32[]{:S(2)}) copy-start(bf16[512,32]{0,1:T(8,128)(2,1)} %param.18) | copy-start | bytes 98308
  7.2 173.2 %copy-start.6 = (bf16[512,32]{0,1:T(8,128)(2,1)S(1)}, bf16[512,32]{0,1:T(8,128)(2,1)}, u32[]{:S(2)}) copy-start(bf16[512,32]{0,1:T(8,128)(2,1)} %param.19) | copy-start | bytes 98308
  7.2 165.2 %all-gather.4.cloned.1.call-start = ((), (), s32[]{:S(2)}) async-start(), calls=%async_computation.1 | async-start | bytes 3194880 | tf_op jit(solution)/shard_map/all_gather | solution.py:33
  8.7 296.4 %all-gather.6.cloned.1.call-start = ((), (), s32[]{:S(2)}) async-start(), calls=%async_computation.2 | async-start | bytes 5324800 | tf_op jit(solution)/shard_map/all_gather | solution.py:33
  175.9 259.2 %all-gather.8.cloned.1.call-start = ((), (), s32[]{:S(2)}) async-start(), calls=%async_computation.3 | async-start | bytes 4259840 | tf_op jit(solution)/shard_map/all_gather | solution.py:44
  176.0 5.8 %collective-permute-start = (bf16[8,512]{1,0:T(8,128)(2,1)S(1)}, bf16[8,512]{1,0:T(8,128)(2,1)S(1)}, u32[]{:S(2)}, u32[]{:S(2)}) collective-permute-start(bf16[8,512]{1,0:T(8,128)(2,1)S(1)} %get-tuple-element.104), channel_id=1, source_target_pairs={{0,4},{4,8},{8,12},{12,16},{16,20},{20,24},{24,28},{28,32},{32,36}... | collective-permute-start | bytes 24584 | tf_op jit(solution)/shard_map/ppermute | solution.py:22
  178.4 5.0 %collective-permute-start.1 = (bf16[8,512]{1,0:T(8,128)(2,1)S(1)}, bf16[8,512]{1,0:T(8,128)(2,1)S(1)}, u32[]{:S(2)}, u32[]{:S(2)}) collective-permute-start(bf16[8,512]{1,0:T(8,128)(2,1)S(1)} %get-tuple-element.105), channel_id=1, source_target_pairs={{4,0},{8,4},{12,8},{16,12},{20,16},{24,20},{28,24},{32,28},{36,32}... | collective-permute-start | bytes 24584 | tf_op jit(solution)/shard_map/ppermute | solution.py:24
  181.1 5.2 %copy-start = (bf16[160,512]{1,0:T(8,128)(2,1)}, bf16[160,512]{1,0:T(8,128)(2,1)S(1)}, u32[]{:S(2)}) copy-start(bf16[160,512]{1,0:T(8,128)(2,1)S(1)} %constant_dynamic-slice_fusion.1) | copy-start | bytes 491524
  326.0 2.2 copy-start.2
  330.5 2.3 copy-start.2
  335.1 2.2 copy-start.2
  339.6 2.3 copy-start.2
  344.1 2.2 copy-start.2
  348.7 2.3 copy-start.2
  353.2 2.3 copy-start.2
  357.8 2.3 copy-start.2
  362.3 2.2 copy-start.2
  371.4 2.2 copy-start.2
  375.9 2.2 copy-start.2
  380.5 2.2 copy-start.2
  385.0 2.3 copy-start.2
  389.6 2.3 copy-start.2
  394.1 2.2 copy-start.2
  398.6 2.3 copy-start.2
  403.2 2.2 copy-start.2
  407.7 2.2 copy-start.2
  412.3 2.3 copy-start.2
  416.1 21.4 %copy-start.1 = (bf16[160,512]{1,0:T(8,128)(2,1)S(1)}, bf16[160,512]{1,0:T(8,128)(2,1)}, u32[]{:S(2)}) copy-start(bf16[160,512]{1,0:T(8,128)(2,1)} %copy-done) | copy-start | bytes 491524
  416.1 21.4 %copy-start.5 = (bf16[176,512]{1,0:T(8,128)(2,1)S(1)}, bf16[176,512]{1,0:T(8,128)(2,1)}, u32[]{:S(2)}) copy-start(bf16[176,512]{1,0:T(8,128)(2,1)} %pad_maximum_fusion) | copy-start | bytes 540676
  416.1 21.4 %copy-start.8 = (f32[160]{0:T(256)S(1)}, f32[160]{0:T(256)}, u32[]{:S(2)}) copy-start(f32[160]{0:T(256)} %subtract_convert_fusion.2) | copy-start | bytes 1924
  437.5 8.7 %copy-start.4 = (f32[1,4,2,160]{3,1,2,0:T(4,128)S(1)}, f32[1,4,2,160]{3,1,2,0:T(4,128)}, u32[]{:S(2)}) copy-start(f32[1,4,2,160]{3,1,2,0:T(4,128)} %get-tuple-element.42) | copy-start | bytes 15364
  442.1 14.6 %all-to-all-start = ((bf16[4,40,2048]{2,1,0:T(8,128)(2,1)}), bf16[4,40,2048]{2,1,0:T(8,128)(2,1)S(1)}, u32[]{:S(2)}, u32[]{:S(2)}) async-start(bf16[4,40,2048]{2,1,0:T(8,128)(2,1)} %bitcast.9), calls=%async_computation | async-start | bytes 1310720 | tf_op jit(solution)/shard_map/all_to_all | solution.py:61
  (21 other events, 14.3 us)
Sparse Core Ops, SparseCore 0:
  10.7 161.6 all-gather.3
  176.0 129.1 all-gather.5
  307.3 127.7 all-gather.7
where the time goes:
time: 466 us; the launch traced here: 464 us
  waiting for transfers between devices  308 us (66%)
  matrix products  72.8 us (16%)
  local copies, waits for them, and re-layouts  32 us (7%)
  other arithmetic  26.8 us (6%)
  between operations  14 us (3%)
  starting transfers between devices  8.71 us (2%)
    all_gather x2, waiting for transfers between devices, side_by_side(): lax.all_gather(both, axis, axis=dim, tiled=True)  280 us
    dot_general x20, matrix products, key_block(): jnp.einsum('qhgmd,khmd->hgmqk', queries, key_blk, preferred_element_type=...  32.7 us
    dot_general x20, matrix products, key_block(): jnp.einsum('hgmqk,khe->hgmqe', weights.astype(jnp.bfloat16), val_blk, pre...  28.4 us
    all_gather x1, waiting for transfers between devices, rows_first(): whole = lax.all_gather(both, axis, axis=0, tiled=True)  17 us
    another operation x20, other arithmetic  16 us
    while x100, local copies, waits for them, and re-layouts  11.8 us
    unnamed x16, local copies, waits for them, and re-layouts  11.2 us
    all_to_all x1, waiting for transfers between devices, sent_and_summed(): lax.all_to_all(blocks, axis, split_axis=0, concat_axis=0, tiled=True)  9.8 us
  transfers between devices with their start and end apart: 6, of which 5 were waited for; matrix products, arithmetic and copies ran while one was open for 23% of the time, Pallas kernels for 0%

commit v1 on v0

--- a/solution.py
+++ b/solution.py
@@ -41,7 +41,9 @@
     turned = [jnp.moveaxis(a, dim, 0) for a, dim in zip(arrays, dims)]
     widths = [t[0].size for t in turned]
     both = jnp.concatenate([t.reshape(-1, w) for t, w in zip(turned, widths)], axis=1)
-    whole = lax.all_gather(both, axis, axis=0, tiled=True)
+    whole = jnp.concatenate(
+        lax.all_to_all(jnp.stack([both] * lax.axis_size(axis)), axis, 0, 0), axis=0
+    )
     blocks = jnp.split(whole, [sum(widths[:k]) for k in range(1, len(widths))], axis=1)
     return tuple(
         (

time: 466 us -> 718 us (1.54)
  waiting for transfers between devices: 308 us -> 544 us
  starting transfers between devices: 8.71 us -> 23 us
    ppermute x1, waiting for transfers between devices: 0.01 us -> 356 us  [extended(): lax.ppermute(tail, axis, [(i, (i + 1) % count) for i in range(ends)])]
    all_gather x2, waiting for transfers between devices: 280 us -> 161 us  [side_by_side(): lax.all_gather(both, axis, axis=dim, tiled=True)]
    ppermute x1, waiting for transfers between devices: 1.63 us -> 19.5 us  [extended(): lax.ppermute(head, axis, [((i + 1) % count, i) for i in range(ends)])]
    all_gather x1 -> x0, waiting for transfers between devices: 17 us -> none  [rows_first(): whole = lax.all_gather(both, axis, axis=0, tiled=True)]
    all_to_all x0 -> x1, starting transfers between devices: none -> 13.8 us  [rows_first(): lax.all_to_all(jnp.stack([both] * lax.axis_size(axis)), axis, 0, 0)]
  transfers between devices with their start and end apart: 6 -> 6, of which waited for: 5 -> 4; matrix products, arithmetic and copies ran while one was open for 23% -> 15% of each run, Pallas kernels for 0% -> 0%
where the time goes in v1:
time: 718 us; the launch traced here: 716 us
  waiting for transfers between devices  544 us (76%)
  matrix products  72.8 us (10%)
  local copies, waits for them, and re-layouts  34.7 us (5%)
  other arithmetic  26.1 us (4%)
  starting transfers between devices  23 us (3%)
  between operations  14.4 us (2%)
    ppermute x1, waiting for transfers between devices, extended(): lax.ppermute(tail, axis, [(i, (i + 1) % count) for i in range(ends)])  356 us
    all_gather x2, waiting for transfers between devices, side_by_side(): lax.all_gather(both, axis, axis=dim, tiled=True)  161 us
    dot_general x20, matrix products, key_block(): jnp.einsum('qhgmd,khmd->hgmqk', queries, key_blk, preferred_element_type=...  32.6 us
    dot_general x20, matrix products, key_block(): jnp.einsum('hgmqk,khe->hgmqe', weights.astype(jnp.bfloat16), val_blk, pre...  28.4 us
    ppermute x1, waiting for transfers between devices, extended(): lax.ppermute(head, axis, [((i + 1) % count, i) for i in range(ends)])  19.5 us
    another operation x20, other arithmetic  16 us
  transfers between devices with their start and end apart: 6, of which 4 were waited for; matrix products, arithmetic and copies ran while one was open for 15% of the time, Pallas kernels for 0%

profile of v1, /device:TPU:33, one launch (start us, length us, event | category | flops | bytes accessed | tf_op | source)
XLA Modules:
  0.0 715.9 jit_solution(3972975601754177202)
XLA Ops:
  11.4 161.0 %all-gather.3.cloned.1.call-done = bf16[2048,768]{1,0:T(8,128)(2,1)} async-done(((bf16[32,768]{1,0:T(8,128)(2,1)}), bf16[2048,768]{1,0:T(8,128)(2,1)}) %all-gather.3.cloned.1.call-update) | async-done | bytes 3145744 | tf_op jit(solution)/shard_map/all_gather | solution.py:33
  175.9 2.6 stack.2
  178.5 13.8 %all-to-all-start = ((bf16[64,32,1024]{2,1,0:T(8,128)(2,1)}), bf16[64,32,1024]{2,1,0:T(8,128)(2,1)}, u32[]{:S(2)}, u32[]{:S(2)}) async-start(bf16[64,32,1024]{2,1,0:T(8,128)(2,1)} %stack.2), calls=%async_computation | async-start | bytes 8388608 | tf_op jit(solution)/shard_map/all_to_all | solution.py:45
  192.4 3.6 collective-permute-start
  196.0 2.0 collective-permute-start.1
  198.6 355.9 %collective-permute-done = bf16[8,512]{1,0:T(8,128)(2,1)S(1)} collective-permute-done((bf16[8,512]{1,0:T(8,128)(2,1)S(1)}, bf16[8,512]{1,0:T(8,128)(2,1)S(1)}, u32[]{:S(2)}, u32[]{:S(2)}) %collective-permute-start) | collective-permute-done | bytes 8224 | tf_op jit(solution)/shard_map/ppermute | solution.py:22
  554.5 19.5 %collective-permute-done.1 = bf16[8,512]{1,0:T(8,128)(2,1)S(1)} collective-permute-done((bf16[8,512]{1,0:T(8,128)(2,1)S(1)}, bf16[8,512]{1,0:T(8,128)(2,1)S(1)}, u32[]{:S(2)}, u32[]{:S(2)}) %collective-permute-start.1) | collective-permute-done | bytes 8224 | tf_op jit(solution)/shard_map/ppermute | solution.py:24
  574.7 2.1 fusion.30
  577.0 3.8 fusion.76
  580.8 4.2 reshape.152
  585.1 11.2 %copy.22 = bf16[20,512,1,2,64]{1,4,3,2,0:T(8,128)(2,1)} copy(bf16[20,512,1,2,64]{4,3,1,0,2:T(2,128)(2,1)} %reshape.152) | data formatting | bytes 5242880
  596.2 90.9 %while.15 = (s32[]{:T(128)}, f32[1,4,2,160]{3,1,2,0:T(4,128)S(1)}, f32[1,4,2,160]{3,1,2,0:T(4,128)}, f32[1,4,2,160,128]{4,3,2,1,0:T(8,128)S(1)}, bf16[20,512,1,2...) while((s32[]{:T(128)}, f32[1,4,2,160]{3,1,2,0:T(4,128)S(1)}, ...), condition=%wide.region_4.5_spmd.clone, body=%wide.region_1.4_spmd.clone.sunk | while | flops 256089600 | bytes 9730209 | solution.py:138
  600.7 1.6 bitcast_reduce_fusion.2
  605.3 1.6 bitcast_reduce_fusion.2
  609.8 1.6 bitcast_reduce_fusion.2
  618.9 1.6 bitcast_reduce_fusion.2
  623.5 1.6 bitcast_reduce_fusion.2
  628.0 1.6 bitcast_reduce_fusion.2
  632.6 1.6 bitcast_reduce_fusion.2
  637.1 1.6 bitcast_reduce_fusion.2
  641.7 1.6 bitcast_reduce_fusion.2
  646.2 1.6 bitcast_reduce_fusion.2
  650.7 1.6 bitcast_reduce_fusion.2
  655.3 1.6 bitcast_reduce_fusion.2
  659.8 1.6 bitcast_reduce_fusion.2
  664.4 1.6 bitcast_reduce_fusion.2
  668.9 1.6 bitcast_reduce_fusion.2
  673.5 1.6 bitcast_reduce_fusion.2
  690.1 2.4 fusion.23
  692.5 4.5 fusion.21
  697.0 3.6 all-to-all-start.1
  701.2 7.0 all-to-all-done.1
  (249 shorter events, 76.9 us)
Async XLA Ops:
  7.2 168.7 %copy-start.7 = (bf16[512,32]{0,1:T(8,128)(2,1)S(1)}, bf16[512,32]{0,1:T(8,128)(2,1)}, u32[]{:S(2)}) copy-start(bf16[512,32]{0,1:T(8,128)(2,1)} %param.18) | copy-start | bytes 98308
  7.2 168.7 %copy-start.6 = (bf16[512,32]{0,1:T(8,128)(2,1)S(1)}, bf16[512,32]{0,1:T(8,128)(2,1)}, u32[]{:S(2)}) copy-start(bf16[512,32]{0,1:T(8,128)(2,1)} %param.19) | copy-start | bytes 98308
  7.2 165.2 %all-gather.3.cloned.1.call-start = ((), (), s32[]{:S(2)}) async-start(), calls=%async_computation.2 | async-start | bytes 3194880 | tf_op jit(solution)/shard_map/all_gather | solution.py:33
  8.7 568.3 %all-gather.5.cloned.1.call-start = ((), (), s32[]{:S(2)}) async-start(), calls=%async_computation.3 | async-start | bytes 5324800 | tf_op jit(solution)/shard_map/all_gather | solution.py:33
  178.5 511.5 %all-to-all-start = ((bf16[64,32,1024]{2,1,0:T(8,128)(2,1)}), bf16[64,32,1024]{2,1,0:T(8,128)(2,1)}, u32[]{:S(2)}, u32[]{:S(2)}) async-start(bf16[64,32,1024]{2,1,0:T(8,128)(2,1)} %stack.2), calls=%async_computation | async-start | bytes 8388608 | tf_op jit(solution)/shard_map/all_to_all | solution.py:45
  192.4 362.2 %collective-permute-start = (bf16[8,512]{1,0:T(8,128)(2,1)S(1)}, bf16[8,512]{1,0:T(8,128)(2,1)S(1)}, u32[]{:S(2)}, u32[]{:S(2)}) collective-permute-start(bf16[8,512]{1,0:T(8,128)(2,1)S(1)} %get-tuple-element.104), channel_id=1, source_target_pairs={{0,4},{4,8},{8,12},{12,16},{16,20},{20,24},{24,28},{28,32},{32,36}... | collective-permute-start | bytes 24584 | tf_op jit(solution)/shard_map/ppermute | solution.py:22
  196.0 378.1 %collective-permute-start.1 = (bf16[8,512]{1,0:T(8,128)(2,1)S(1)}, bf16[8,512]{1,0:T(8,128)(2,1)S(1)}, u32[]{:S(2)}, u32[]{:S(2)}) collective-permute-start(bf16[8,512]{1,0:T(8,128)(2,1)S(1)} %get-tuple-element.105), channel_id=1, source_target_pairs={{4,0},{8,4},{12,8},{16,12},{20,16},{24,20},{28,24},{32,28},{36,32}... | collective-permute-start | bytes 24584 | tf_op jit(solution)/shard_map/ppermute | solution.py:24
  198.0 379.0 %copy-start = (bf16[160,512]{1,0:T(8,128)(2,1)}, bf16[160,512]{1,0:T(8,128)(2,1)S(1)}, u32[]{:S(2)}) copy-start(bf16[160,512]{1,0:T(8,128)(2,1)S(1)} %constant_dynamic-slice_fusion.1) | copy-start | bytes 491524
  597.9 2.2 copy-start.2
  602.4 2.2 copy-start.2
  611.5 2.3 copy-start.2
  616.0 2.3 copy-start.2
  620.6 2.3 copy-start.2
  625.1 2.3 copy-start.2
  629.7 2.3 copy-start.2
  634.2 2.3 copy-start.2
  638.8 2.3 copy-start.2
  643.3 2.3 copy-start.2
  647.9 2.3 copy-start.2
  652.4 2.3 copy-start.2
  657.0 2.3 copy-start.2
  661.5 2.3 copy-start.2
  666.0 2.3 copy-start.2
  670.6 2.3 copy-start.2
  675.1 2.3 copy-start.2
  679.7 2.3 copy-start.2
  684.2 2.3 copy-start.2
  688.1 4.4 copy-start.1
  688.1 4.4 copy-start.5
  688.1 4.4 copy-start.8
  692.5 8.1 %copy-start.4 = (f32[1,4,2,160]{3,1,2,0:T(4,128)S(1)}, f32[1,4,2,160]{3,1,2,0:T(4,128)}, u32[]{:S(2)}) copy-start(f32[1,4,2,160]{3,1,2,0:T(4,128)} %get-tuple-element.42) | copy-start | bytes 15364
  697.0 11.2 %all-to-all-start.1 = ((bf16[4,40,2048]{2,1,0:T(8,128)(2,1)}), bf16[4,40,2048]{2,1,0:T(8,128)(2,1)S(1)}, u32[]{:S(2)}, u32[]{:S(2)}) async-start(bf16[4,40,2048]{2,1,0:T(8,128)(2,1)} %bitcast.10), calls=%async_computation.1 | async-start | bytes 1310720 | tf_op jit(solution)/shard_map/all_to_all | solution.py:63
  (21 other events, 14.3 us)
Sparse Core Ops, SparseCore 0:
  10.7 161.6 all-gather.2
  176.0 311.4 all-gather.4
